TPU v7x, 32 devices: a whole 2x2x4 slice. The times are simulated.
32 devices in a mesh: kv: 16 (over z, x, core), tp: 2 (over y).
Axes of the slice: x: 2, y: 2, z: 4, core: 2. Of those that a mesh axis runs over, the one named last changes fastest.
Arguments:
- queries: bfloat16 [2048, 4096], P('kv', 'tp'), may hold values from -6 to 6
- keys: bfloat16 [2048, 512], P('kv', 'tp'), may hold values from -6 to 6
- values: bfloat16 [2048, 512], P('kv', 'tp'), may hold values from -6 to 6
- logsum: float32 [2048, 32], P('kv', 'tp'), may hold values from 2 to 6
- out_grad: bfloat16 [2048, 4096], P('kv', 'tp'), may hold values from -6 to 6
- normed_input: bfloat16 [2048, 4096], P('kv', 'tp'), may hold values from -6 to 6
- chosen: int32 [32, 16], P('kv'), may hold values from 0 to 63, as said below
Outputs:
- query_grad: float32 [2048, 4096], P('kv', 'tp')
- key_grad: float32 [2048, 512], P('kv', 'tp')
- value_grad: float32 [2048, 512], P('kv', 'tp')
- value_weight_grad: float32 [4096, 512], P('kv', 'tp')
Inputs may be any that keep to these rules, and one draw needn't show every extreme that they name: `chosen`: each row r names 16 distinct key blocks, among them block 0 and the blocks r * 2 to r * 2 + 64 / 32 - 1 that hold the query block's own positions. The rows of one device (aligned runs of 2 rows) name at most one block of any other device's 128 / 32 blocks. Blocks after the query block may be named; their keys are masked.
All inputs are finite; a program needn't handle non-finite values.
Results may differ from a plain program's by a relative error of at most 0.008.
Values may be sent and summed in bfloat16 or wider, within the bound.
A program may use at most 64 MiB of HBM per device.

v0:
```python
import jax
import jax.numpy as jnp
from jax import lax
from jax.sharding import PartitionSpec as P

HD = 128
QB = 64
KB = 32
NSEL = 16


def local(queries, keys, values, logsum, out_grad, normed_input, chosen):
    devices = lax.axis_size("kv")
    here = lax.axis_index("kv")
    tok = keys.shape[0]
    kv_cols = keys.shape[1]
    kv_heads = kv_cols // HD
    group = queries.shape[1] // kv_cols
    kblocks = tok // KB
    qblocks = tok // QB
    span = NSEL * KB
    scale = HD ** (-0.5)
    owner = chosen // kblocks
    within = chosen % kblocks
    remote = owner != here
    peers = jnp.arange(devices, dtype=jnp.int32)
    named = (owner[:, :, None] == peers[None, None, :]) & remote[:, :, None]
    wanted = jnp.max(jnp.where(named, within[:, :, None] + 1, 0), axis=(0, 1))
    asked = (
        lax.all_to_all(
            wanted.reshape(devices, 1), "kv", split_axis=0, concat_axis=0, tiled=True
        ).reshape(devices)
        - 1
    )
    key_blocks = keys.reshape(kblocks, KB, kv_cols)
    value_blocks = values.reshape(kblocks, KB, kv_cols)
    taken = jnp.maximum(asked, 0)
    live = (asked >= 0)[:, None, None]
    send_keys = jnp.where(live, key_blocks[taken], jnp.zeros((), keys.dtype))
    send_values = jnp.where(live, value_blocks[taken], jnp.zeros((), values.dtype))
    got_keys, got_values = (
        lax.all_to_all(send_keys, "kv", split_axis=0, concat_axis=0, tiled=True),
        lax.all_to_all(send_values, "kv", split_axis=0, concat_axis=0, tiled=True),
    )
    pool_keys = jnp.concatenate([key_blocks, got_keys], axis=0)
    pool_values = jnp.concatenate([value_blocks, got_values], axis=0)
    slot = jnp.where(remote, kblocks + owner, within)
    sel_keys = pool_keys[slot].reshape(qblocks, span, kv_heads, HD)
    sel_values = pool_values[slot].reshape(qblocks, span, kv_heads, HD)
    query_rows = queries.reshape(qblocks, QB, kv_heads, group, HD)
    dout = out_grad.reshape(qblocks, QB, kv_heads, group, HD)
    lse = logsum.reshape(qblocks, QB, kv_heads, group)
    scores = (
        jnp.einsum("bqngd,bjnd->bqngj", query_rows, sel_keys, preferred_element_type=jnp.float32)
        * scale
    )
    qpos = here * tok + jnp.arange(tok, dtype=jnp.int32).reshape(qblocks, QB)
    kpos = (chosen[:, :, None] * KB + jnp.arange(KB, dtype=jnp.int32)[None, None, :]).reshape(
        qblocks, span
    )
    valid = (kpos[:, None, :] <= qpos[:, :, None])[:, :, None, None, :]
    prob = jnp.where(valid, jnp.exp(scores - lse[..., None]), 0.0)
    dprob = jnp.einsum("bqngd,bjnd->bqngj", dout, sel_values, preferred_element_type=jnp.float32)
    delta = jnp.sum(prob * dprob, axis=-1, keepdims=True)
    dscore = (prob * (dprob - delta)).astype(jnp.bfloat16)
    prob_low = prob.astype(jnp.bfloat16)
    query_grad = (
        jnp.einsum("bqngj,bjnd->bqngd", dscore, sel_keys, preferred_element_type=jnp.float32)
        * scale
    )
    query_grad = query_grad.reshape(tok, queries.shape[1])
    key_part = (
        jnp.einsum("bqngj,bqngd->bjnd", dscore, query_rows, preferred_element_type=jnp.float32)
        * scale
    )
    value_part = jnp.einsum("bqngj,bqngd->bjnd", prob_low, dout, preferred_element_type=jnp.float32)
    entries = qblocks * NSEL
    pool_size = kblocks + devices
    onehot = (slot.reshape(entries, 1) == jnp.arange(pool_size, dtype=jnp.int32)[None, :]).astype(
        jnp.float32
    )
    key_sum = jnp.dot(
        onehot.T,
        key_part.reshape(entries, KB * kv_cols),
        precision=lax.Precision.HIGHEST,
        preferred_element_type=jnp.float32,
    )
    value_sum = jnp.dot(
        onehot.T,
        value_part.reshape(entries, KB * kv_cols),
        precision=lax.Precision.HIGHEST,
        preferred_element_type=jnp.float32,
    )
    back_keys = key_sum[kblocks:].reshape(devices, KB, kv_cols)
    back_values = value_sum[kblocks:].reshape(devices, KB, kv_cols)
    ret_keys, ret_values = (
        lax.all_to_all(back_keys, "kv", split_axis=0, concat_axis=0, tiled=True),
        lax.all_to_all(back_values, "kv", split_axis=0, concat_axis=0, tiled=True),
    )
    home = (asked[:, None] == jnp.arange(kblocks, dtype=jnp.int32)[None, :]).astype(jnp.float32)
    key_grad = key_sum[:kblocks] + jnp.dot(
        home.T,
        ret_keys.reshape(devices, KB * kv_cols),
        precision=lax.Precision.HIGHEST,
        preferred_element_type=jnp.float32,
    )
    value_grad = value_sum[:kblocks] + jnp.dot(
        home.T,
        ret_values.reshape(devices, KB * kv_cols),
        precision=lax.Precision.HIGHEST,
        preferred_element_type=jnp.float32,
    )
    key_grad = key_grad.reshape(tok, kv_cols)
    value_grad = value_grad.reshape(tok, kv_cols)
    value_low = value_grad.astype(jnp.bfloat16)
    full_input = lax.all_gather(normed_input, "tp", axis=1, tiled=True)
    weight_grad = lax.psum_scatter(
        jnp.einsum("td,tc->dc", full_input, value_low, preferred_element_type=jnp.float32),
        "kv",
        scatter_dimension=0,
        tiled=True,
    )
    return (query_grad, key_grad, value_grad, weight_grad)


def solution(mesh):
    in_specs = (
        P("kv", "tp"),
        P("kv", "tp"),
        P("kv", "tp"),
        P("kv", "tp"),
        P("kv", "tp"),
        P("kv", "tp"),
        P("kv", None),
    )
    out_specs = (P("kv", "tp"), P("kv", "tp"), P("kv", "tp"), P("kv", "tp"))
    return jax.shard_map(local, mesh=mesh, in_specs=in_specs, out_specs=out_specs, check_vma=False)
```

profile of v0, /device:TPU:0, one launch (start us, length us, event | category | flops | bytes accessed | tf_op | source)
XLA Modules:
  0.0 171.1 jit_solution(7793433736477169849)
XLA Ops:
  7.2 0.0 copy-start.4
  7.2 0.8 compare_select_fusion
  8.0 0.1 select_reduce_fusion
  8.1 0.7 copy.55
  8.7 7.4 %all-to-all-start = ((s32[16,1,1]{2,1,0:T(1,128)}), s32[16,1,1]{2,1,0:T(1,128)S(1)}, u32[]{:S(2)}, u32[]{:S(2)}) async-start(s32[16,1,1]{2,1,0:T(1,128)} %copy.55), calls=%async_computation | async-start | bytes 16384 | tf_op jit(solution)/shard_map/all_to_all | solution.py:30
  16.1 0.1 reshape.149
  16.2 6.3 %all-to-all-done = s32[16,1,1]{2,1,0:T(1,128)S(1)} async-done(((s32[16,1,1]{2,1,0:T(1,128)}), s32[16,1,1]{2,1,0:T(1,128)S(1)}, u32[]{:S(2)}, u32[]{:S(2)}) %all-to-all-start) | async-done | bytes 96 | tf_op jit(solution)/shard_map/all_to_all | solution.py:30
  22.5 0.7 fusion.35
  23.2 1.4 gather_fusion.2
  24.6 1.4 gather_fusion
  26.0 0.4 compare_reduce_fusion
  26.4 0.8 broadcast_select_fusion.1
  27.2 3.5 %all-to-all-start.1 = ((bf16[16,32,256]{2,1,0:T(8,128)(2,1)}), bf16[16,32,256]{2,1,0:T(8,128)(2,1)S(1)}, u32[]{:S(2)}, u32[]{:S(2)}) async-start(bf16[16,32,256]{2,1,0:T(8,128)(2,1)} %get-tuple-element.31), calls=%async_computation.1 | async-start | bytes 524288 | tf_op jit(solution)/shard_map/all_to_all | solution.py:42
  30.8 0.1 eq.46
  30.8 0.1 add.89
  30.9 0.1 add.86
  31.0 0.1 add.87
  31.1 0.8 sub.31
  31.9 1.1 copy.79
  33.0 0.1 copy.80
  33.1 0.0 copy-start.2
  33.2 0.1 broadcast_compare_fusion
  33.3 7.4 %all-to-all-done.1 = bf16[16,32,256]{2,1,0:T(8,128)(2,1)S(1)} async-done(((bf16[16,32,256]{2,1,0:T(8,128)(2,1)}), bf16[16,32,256]{2,1,0:T(8,128)(2,1)S(1)}, u32[]{:S(2)}, u32[]{:S(2)}) %all-to-all-start.1) | async-done | bytes 262176 | tf_op jit(solution)/shard_map/all_to_all | solution.py:42
  40.8 0.6 gather_fusion.1
  41.3 0.1 reshape.122
  41.5 0.7 fusion.20
  42.2 2.0 %copy-done = f32[2,2,512,64,8]{2,3,4,1,0:T(8,128)} copy-done((f32[2,2,512,64,8]{2,3,4,1,0:T(8,128)}, f32[2,2,512,64,8]{2,3,4,1,0:T(8,128)S(1)}, u32[]{:S(2)}) %copy-start) | copy-done | bytes 4194328
  44.2 1.8 %fusion.14 = f32[2,512,2,128]{3,1,2,0:T(8,128)S(1)} fusion(f32[2,2,512,64,8]{2,3,4,1,0:T(8,128)S(1)} %fusion.20, f32[2,64,2,8]{1,3,2,0:T(8,128)S(1)} %copy.58, pred[2,64,512]{2,1,0:T(8,128)(4,1)S(1)} %broadcast_compare_fusion, bf16[2,64,2,8,128]{4,3,2,1,0:T(8,128)(2,1)S(1)} %bitcast.77), kind=kOutput, calls=%fused_computation.24 | convolution fusion | flops 272629760 | bytes 5840896 | tf_op jit(solution)/shard_map/bqngj,bqngd->bjnd/dot_general | solution.py:76
  46.0 0.8 copy.66
  46.8 0.8 reshape.135
  47.6 0.6 fusion.28
  48.3 1.0 copy.83
  49.3 3.6 %all-to-all-start.4 = ((f32[16,32,256]{2,1,0:T(8,128)}), f32[16,32,256]{2,1,0:T(8,128)S(1)}, u32[]{:S(2)}, u32[]{:S(2)}) async-start(f32[16,32,256]{2,1,0:T(8,128)} %bitcast.30), calls=%async_computation.4 | async-start | bytes 1048576 | tf_op jit(solution)/shard_map/all_to_all | solution.py:98
  52.8 0.0 all-gather.2.cloned.1.call-start
  52.9 0.7 all-gather.2.cloned.1.call-update
  53.6 0.0 reduce-scatter.2.cloned.1.call-start
  53.6 13.5 %all-to-all-done.4 = f32[16,32,256]{2,1,0:T(8,128)S(1)} async-done(((f32[16,32,256]{2,1,0:T(8,128)}), f32[16,32,256]{2,1,0:T(8,128)S(1)}, u32[]{:S(2)}, u32[]{:S(2)}) %all-to-all-start.4) | async-done | bytes 524320 | tf_op jit(solution)/shard_map/all_to_all | solution.py:98
  67.1 0.3 copy.84
  67.4 0.4 convolution_add_fusion
  67.8 0.1 reshape.138
  67.9 9.9 %all-gather.2.cloned.1.call-done = bf16[128,4096]{1,0:T(8,128)(2,1)} async-done(((bf16[128,2048]{1,0:T(8,128)(2,1)}), bf16[128,4096]{1,0:T(8,128)(2,1)}) %all-gather.2.cloned.1.call-update) | async-done | bytes 1048592 | tf_op jit(solution)/shard_map/all_gather | solution.py:116
  77.8 3.9 %convolution_bitcast_fusion = f32[4096,256]{0,1:T(8,128)} fusion(bf16[128,4096]{1,0:T(8,128)(2,1)} %all-gather.2.cloned.1.call-done, f32[128,256]{1,0:T(8,128)S(1)} %reshape.138), kind=kOutput, calls=%fused_computation.6 | convolution fusion | flops 268468224 | bytes 5373952 | tf_op jit(solution)/shard_map/td,tc->dc/dot_general | solution.py:118
  81.7 0.0 reduce-scatter.2.cloned.1.call-update
  81.7 15.6 %all_to_all.29 = bf16[16,32,256]{2,1,0:T(8,128)(2,1)S(1)} all-to-all(bf16[16,32,256]{2,1,0:T(8,128)(2,1)S(1)} %get-tuple-element.32), channel_id=1, replica_groups=mesh['kv'=16,'tp'=2] {'kv'}, dimensions={0} | all-to-all | bytes 524288 | tf_op jit(solution)/shard_map/all_to_all | solution.py:43
  97.3 0.6 gather_fusion.3
  97.9 0.1 reshape.128
  98.1 3.6 %fusion = (f32[2,64,2,8]{1,3,2,0:T(8,128)S(1)}, f32[2,2,512,64,8]{2,3,4,1,0:T(8,128)S(1)}) fusion(f32[2,2,512,64,8]{2,3,4,1,0:T(8,128)} %copy-done, f32[2,64,2,8]{1,3,2,0:T(8,128)S(1)} %copy.58, pred[2,64,512]{2,1,0:T(8,128)(4,1)S(1)} %broadcast_compare_fusion, bf16[2,64,2,8,128]{4,3,2,1,0:T(8,128)(2,1)S(1)} %bitcast.78, ...), kind=kOutput, calls=%fused_computation.9 | convolution fusion | flops 273676288 | bytes 9519104 | tf_op jit(solution)/shard_map/bqngd,bjnd->bqngj/dot_general | solution.py:63
  101.7 0.3 copy-done.1
  101.9 1.5 fusion.2
  103.5 0.9 fusion.13
  104.4 1.8 %copy.64 = f32[2,512,2,128]{3,2,1,0:T(2,128)} copy(f32[2,512,2,128]{3,1,2,0:T(8,128)S(1)} %fusion.13) | data formatting | bytes 2097152 | tf_op jit(solution)/shard_map/mul | solution.py:73
  106.2 3.0 %reshape.131 = f32[32,8192]{1,0:T(8,128)} reshape(f32[2,512,2,128]{3,2,1,0:T(2,128)} %copy.64) | data formatting | bytes 2097152 | tf_op jit(solution)/shard_map/reshape | solution.py:84
  109.2 1.8 %fusion.29 = f32[20,8192]{1,0:T(8,128)S(1)} fusion(f32[32,8192]{1,0:T(8,128)} %reshape.131, s32[32]{0:T(128)S(1)} %eq.46), kind=kOutput, calls=%fused_computation.45 | convolution fusion | flops 62915200 | bytes 1704064 | tf_op jit(solution)/shard_map/dot_general | solution.py:82
  111.1 1.0 copy.81
  112.0 4.2 %all-to-all-start.3 = ((f32[16,32,256]{2,1,0:T(8,128)}), f32[16,32,256]{2,1,0:T(8,128)}, u32[]{:S(2)}, u32[]{:S(2)}) async-start(f32[16,32,256]{2,1,0:T(8,128)} %bitcast.81), calls=%async_computation.3 | async-start | bytes 1048576 | tf_op jit(solution)/shard_map/all_to_all | solution.py:97
  116.3 0.7 fusion.17
  117.0 0.6 copy.62
  117.6 1.1 reshape.130
  118.8 17.0 %all-to-all-done.3 = f32[16,32,256]{2,1,0:T(8,128)} async-done(((f32[16,32,256]{2,1,0:T(8,128)}), f32[16,32,256]{2,1,0:T(8,128)}, u32[]{:S(2)}, u32[]{:S(2)}) %all-to-all-start.3) | async-done | bytes 524320 | tf_op jit(solution)/shard_map/all_to_all | solution.py:97
  135.8 1.4 copy.82
  137.1 0.4 convolution_add_fusion.1
  137.5 0.7 reshape.134
  138.3 24.2 %reduce-scatter.2.cloned.1.call-done = f32[256,256]{0,1:T(8,128)} async-done(((f32[4096,256]{0,1:T(8,128)}), f32[256,256]{0,1:T(8,128)}) %reduce-scatter.2.cloned.1.call-update) | async-done | bytes 262160 | tf_op jit(solution)/shard_map/reduce_scatter | solution.py:117
  162.4 1.8 %copy.67 = f32[256,256]{1,0:T(8,128)} copy(f32[256,256]{0,1:T(8,128)} %reduce-scatter.2.cloned.1.call-done) | data formatting | bytes 524288
  (23 shorter events, 0.2 us)
Async XLA Ops:
  7.2 33.6 %copy-start.4 = (bf16[128,256]{1,0:T(8,128)(2,1)S(1)}, bf16[128,256]{1,0:T(8,128)(2,1)}, u32[]{:S(2)}) copy-start(bf16[128,256]{1,0:T(8,128)(2,1)} %param.8) | copy-start | bytes 196612
  7.2 25.8 %copy-start.6 = (bf16[128,2048]{1,0:T(8,128)(2,1)S(1)}, bf16[128,2048]{1,0:T(8,128)(2,1)}, u32[]{:S(2)}) copy-start(bf16[128,2048]{1,0:T(8,128)(2,1)} %param.11) | copy-start | bytes 1572868
  8.7 13.8 %all-to-all-start = ((s32[16,1,1]{2,1,0:T(1,128)}), s32[16,1,1]{2,1,0:T(1,128)S(1)}, u32[]{:S(2)}, u32[]{:S(2)}) async-start(s32[16,1,1]{2,1,0:T(1,128)} %copy.55), calls=%async_computation | async-start | bytes 16384 | tf_op jit(solution)/shard_map/all_to_all | solution.py:30
  27.2 13.5 %all-to-all-start.1 = ((bf16[16,32,256]{2,1,0:T(8,128)(2,1)}), bf16[16,32,256]{2,1,0:T(8,128)(2,1)S(1)}, u32[]{:S(2)}, u32[]{:S(2)}) async-start(bf16[16,32,256]{2,1,0:T(8,128)(2,1)} %get-tuple-element.31), calls=%async_computation.1 | async-start | bytes 524288 | tf_op jit(solution)/shard_map/all_to_all | solution.py:42
  33.1 9.1 %copy-start.2 = (bf16[16,8,16,128]{3,2,1,0:T(8,128)(2,1)}, bf16[16,8,16,128]{3,2,1,0:T(8,128)(2,1)S(1)}, u32[]{:S(2)}) copy-start(bf16[16,8,16,128]{3,2,1,0:T(8,128)(2,1)S(1)} %copy.80) | copy-start | bytes 1572868
  42.2 2.0 %copy-start = (f32[2,2,512,64,8]{2,3,4,1,0:T(8,128)}, f32[2,2,512,64,8]{2,3,4,1,0:T(8,128)S(1)}, u32[]{:S(2)}) copy-start(f32[2,2,512,64,8]{2,3,4,1,0:T(8,128)S(1)} %fusion.20) | copy-start | bytes 12582916
  49.3 17.8 %all-to-all-start.4 = ((f32[16,32,256]{2,1,0:T(8,128)}), f32[16,32,256]{2,1,0:T(8,128)S(1)}, u32[]{:S(2)}, u32[]{:S(2)}) async-start(f32[16,32,256]{2,1,0:T(8,128)} %bitcast.30), calls=%async_computation.4 | async-start | bytes 1048576 | tf_op jit(solution)/shard_map/all_to_all | solution.py:98
  52.8 25.0 %all-gather.2.cloned.1.call-start = ((), (), s32[]{:S(2)}) async-start(), calls=%async_computation.6 | async-start | bytes 1572864 | tf_op jit(solution)/shard_map/all_gather | solution.py:116
  53.6 108.9 %reduce-scatter.2.cloned.1.call-start = ((), (), s32[]{:S(2)}) async-start(), calls=%async_computation.7 | async-start | bytes 4456448 | tf_op jit(solution)/shard_map/reduce_scatter | solution.py:117
  67.9 9.9 %copy-start.7 = (f32[128,256]{1,0:T(8,128)}, f32[128,256]{1,0:T(8,128)S(1)}, u32[]{:S(2)}) copy-start(f32[128,256]{1,0:T(8,128)S(1)} %reshape.138) | copy-start | bytes 393220
  67.9 29.4 %copy-start.5 = (bf16[128,256]{1,0:T(8,128)(2,1)S(1)}, bf16[128,256]{1,0:T(8,128)(2,1)}, u32[]{:S(2)}) copy-start(bf16[128,256]{1,0:T(8,128)(2,1)} %param.9) | copy-start | bytes 196612
  81.7 16.3 %copy-start.3 = (bf16[16,8,16,128]{3,2,1,0:T(8,128)(2,1)S(1)}, bf16[16,8,16,128]{3,2,1,0:T(8,128)(2,1)}, u32[]{:S(2)}) copy-start(bf16[16,8,16,128]{3,2,1,0:T(8,128)(2,1)} %copy-done.2) | copy-start | bytes 1572868
  98.1 3.9 %copy-start.1 = (f32[2,2,512,64,8]{2,3,4,1,0:T(8,128)S(1)}, f32[2,2,512,64,8]{2,3,4,1,0:T(8,128)}, u32[]{:S(2)}) copy-start(f32[2,2,512,64,8]{2,3,4,1,0:T(8,128)} %copy-done) | copy-start | bytes 12582916
  112.0 23.7 %all-to-all-start.3 = ((f32[16,32,256]{2,1,0:T(8,128)}), f32[16,32,256]{2,1,0:T(8,128)}, u32[]{:S(2)}, u32[]{:S(2)}) async-start(f32[16,32,256]{2,1,0:T(8,128)} %bitcast.81), calls=%async_computation.3 | async-start | bytes 1048576 | tf_op jit(solution)/shard_map/all_to_all | solution.py:97
Sparse Core Ops, SparseCore 0:
  55.2 22.5 all-gather.1
  81.9 80.5 reduce-scatter.1
where the time goes:
time: 172 us; the launch traced here: 171 us
  waiting for transfers between devices  78.9 us (46%)
  local copies, waits for them, and re-layouts  24.1 us (14%)
  starting transfers between devices  18.8 us (11%)
  blocking collectives  15.6 us (9%)
  matrix products  14.8 us (9%)
  between operations  14.4 us (8%)
  other arithmetic  4.43 us (3%)
    reduce_scatter x1, waiting for transfers between devices, local(): lax.psum_scatter(jnp.einsum('td,tc->dc', full_input, value_low, preferred...  24.2 us
    all_to_all x1, waiting for transfers between devices, local(): lax.all_to_all(back_keys, 'kv', split_axis=0, concat_axis=0, tiled=True)  17 us
    all_to_all x1, blocking collectives, local(): lax.all_to_all(send_values, 'kv', split_axis=0, concat_axis=0, tiled=True)  15.6 us
    all_to_all x1, waiting for transfers between devices, local(): lax.all_to_all(back_values, 'kv', split_axis=0, concat_axis=0, tiled=True)  13.5 us
    all_gather x1, waiting for transfers between devices, local(): full_input = lax.all_gather(normed_input, 'tp', axis=1, tiled=True)  9.91 us
    unnamed x23, local copies, waits for them, and re-layouts  8.89 us
    all_to_all x1, waiting for transfers between devices, local(): lax.all_to_all(send_keys, 'kv', split_axis=0, concat_axis=0, tiled=True)  7.44 us
    all_to_all x1, starting transfers between devices, local(): lax.all_to_all(wanted.reshape(devices, 1), 'kv', split_axis=0, concat_axi...  7.39 us
  transfers between devices with their start and end apart: 6, of which 6 were waited for; matrix products, arithmetic and copies ran while one was open for 13% of the time, Pallas kernels for 0%

commit v1 on v0

--- a/solution.py
+++ b/solution.py
@@ -113,7 +113,8 @@
     key_grad = key_grad.reshape(tok, kv_cols)
     value_grad = value_grad.reshape(tok, kv_cols)
     value_low = value_grad.astype(jnp.bfloat16)
-    full_input = lax.all_gather(normed_input, "tp", axis=1, tiled=True)
+    pieces = lax.all_gather(normed_input, "tp")
+    full_input = jnp.concatenate(pieces, axis=1)
     weight_grad = lax.psum_scatter(
         jnp.einsum("td,tc->dc", full_input, value_low, preferred_element_type=jnp.float32),
         "kv",

time: 172 us -> 162 us (0.942)
  waiting for transfers between devices: 78.9 us -> 68.4 us
  local copies, waits for them, and re-layouts: 24.1 us -> 26.4 us
    all_gather x1, waiting for transfers between devices: 9.91 us -> 0.02 us  [local(): pieces = lax.all_gather(normed_input, 'tp')]
    unnamed x23 -> x27, local copies, waits for them, and re-layouts: 8.89 us -> 8.9 us
  transfers between devices with their start and end apart: 6 -> 6, of which waited for: 6 -> 5; matrix products, arithmetic and copies ran while one was open for 13% -> 23% of each run, Pallas kernels for 0% -> 0%
where the time goes in v1:
time: 162 us; the launch traced here: 161 us
  waiting for transfers between devices  68.4 us (42%)
  local copies, waits for them, and re-layouts  26.4 us (16%)
  starting transfers between devices  18.8 us (12%)
  between operations  14.4 us (9%)
  matrix products  14.3 us (9%)
  blocking collectives  14 us (9%)
  other arithmetic  4.37 us (3%)
    reduce_scatter x1, waiting for transfers between devices, local(): lax.psum_scatter(jnp.einsum('td,tc->dc', full_input, value_low, preferred...  24.4 us
    all_to_all x1, waiting for transfers between devices, local(): lax.all_to_all(back_keys, 'kv', split_axis=0, concat_axis=0, tiled=True)  17 us
    all_to_all x1, blocking collectives, local(): lax.all_to_all(send_values, 'kv', split_axis=0, concat_axis=0, tiled=True)  14 us
    all_to_all x1, waiting for transfers between devices, local(): lax.all_to_all(back_values, 'kv', split_axis=0, concat_axis=0, tiled=True)  12.5 us
    unnamed x27, local copies, waits for them, and re-layouts  8.9 us
    all_to_all x1, waiting for transfers between devices, local(): lax.all_to_all(send_keys, 'kv', split_axis=0, concat_axis=0, tiled=True)  7.43 us
    all_to_all x1, starting transfers between devices, local(): lax.all_to_all(wanted.reshape(devices, 1), 'kv', split_axis=0, concat_axi...  7.39 us
    all_to_all x1, waiting for transfers between devices, local(): lax.all_to_all(wanted.reshape(devices, 1), 'kv', split_axis=0, concat_axi...  6.27 us
  transfers between devices with their start and end apart: 6, of which 5 were waited for; matrix products, arithmetic and copies ran while one was open for 23% of the time, Pallas kernels for 0%

profile of v1, /device:TPU:0, one launch (start us, length us, event | category | flops | bytes accessed | tf_op | source)
XLA Modules:
  0.0 160.7 jit_solution(11871907945134451082)
XLA Ops:
  7.2 0.0 all-gather.3.cloned.1.call-start
  7.2 0.7 all-gather.3.cloned.1.call-update
  7.9 0.7 compare_select_fusion
  8.6 0.1 select_reduce_fusion
  8.7 0.7 copy.70
  9.4 7.4 %all-to-all-start = ((s32[16,1,1]{2,1,0:T(1,128)}), s32[16,1,1]{2,1,0:T(1,128)S(1)}, u32[]{:S(2)}, u32[]{:S(2)}) async-start(s32[16,1,1]{2,1,0:T(1,128)} %copy.70), calls=%async_computation | async-start | bytes 16384 | tf_op jit(solution)/shard_map/all_to_all | solution.py:30
  16.8 0.1 reshape.158
  16.9 6.3 %all-to-all-done = s32[16,1,1]{2,1,0:T(1,128)S(1)} async-done(((s32[16,1,1]{2,1,0:T(1,128)}), s32[16,1,1]{2,1,0:T(1,128)S(1)}, u32[]{:S(2)}, u32[]{:S(2)}) %all-to-all-start) | async-done | bytes 96 | tf_op jit(solution)/shard_map/all_to_all | solution.py:30
  23.2 0.7 fusion.34
  23.8 1.4 gather_fusion.2
  25.3 1.4 gather_fusion
  26.7 0.4 compare_reduce_fusion
  27.1 0.8 broadcast_select_fusion.1
  27.9 3.5 %all-to-all-start.1 = ((bf16[16,32,256]{2,1,0:T(8,128)(2,1)}), bf16[16,32,256]{2,1,0:T(8,128)(2,1)S(1)}, u32[]{:S(2)}, u32[]{:S(2)}) async-start(bf16[16,32,256]{2,1,0:T(8,128)(2,1)} %get-tuple-element.35), calls=%async_computation.1 | async-start | bytes 524288 | tf_op jit(solution)/shard_map/all_to_all | solution.py:42
  31.4 0.1 eq.46
  31.5 0.1 add.89
  31.6 0.1 add.86
  31.7 0.1 add.87
  31.8 0.8 sub.31
  32.5 1.1 copy.95
  33.7 0.1 copy.96
  33.8 0.0 copy-start.4
  33.9 0.1 broadcast_compare_fusion
  34.0 7.4 %all-to-all-done.1 = bf16[16,32,256]{2,1,0:T(8,128)(2,1)S(1)} async-done(((bf16[16,32,256]{2,1,0:T(8,128)(2,1)}), bf16[16,32,256]{2,1,0:T(8,128)(2,1)S(1)}, u32[]{:S(2)}, u32[]{:S(2)}) %all-to-all-start.1) | async-done | bytes 262176 | tf_op jit(solution)/shard_map/all_to_all | solution.py:42
  41.4 0.6 gather_fusion.1
  42.0 0.1 reshape.129
  42.2 0.7 fusion.20
  42.9 1.9 %copy-done = f32[2,2,512,64,8]{2,3,4,1,0:T(8,128)} copy-done((f32[2,2,512,64,8]{2,3,4,1,0:T(8,128)}, f32[2,2,512,64,8]{2,3,4,1,0:T(8,128)S(1)}, u32[]{:S(2)}) %copy-start) | copy-done | bytes 4194328
  44.8 1.8 %fusion.14 = f32[2,512,2,128]{3,1,2,0:T(8,128)S(1)} fusion(f32[2,2,512,64,8]{2,3,4,1,0:T(8,128)S(1)} %fusion.20, f32[2,64,2,8]{1,3,2,0:T(8,128)S(1)} %copy.73, pred[2,64,512]{2,1,0:T(8,128)(4,1)S(1)} %broadcast_compare_fusion, bf16[2,64,2,8,128]{4,3,2,1,0:T(8,128)(2,1)S(1)} %bitcast.83), kind=kOutput, calls=%fused_computation.24 | convolution fusion | flops 272629760 | bytes 5840896 | tf_op jit(solution)/shard_map/bqngj,bqngd->bjnd/dot_general | solution.py:76
  46.6 0.8 copy.81
  47.4 0.8 reshape.142
  48.3 0.6 fusion.27
  49.0 1.0 copy.99
  49.9 3.6 %all-to-all-start.4 = ((f32[16,32,256]{2,1,0:T(8,128)}), f32[16,32,256]{2,1,0:T(8,128)S(1)}, u32[]{:S(2)}, u32[]{:S(2)}) async-start(f32[16,32,256]{2,1,0:T(8,128)} %bitcast.34), calls=%async_computation.4 | async-start | bytes 1048576 | tf_op jit(solution)/shard_map/all_to_all | solution.py:98
  53.5 0.0 reduce-scatter.2.cloned.1.call-start
  53.6 0.0 all-gather.3.cloned.1.call-done
  53.6 1.6 %copy.82 = bf16[128,2,2048]{0,2,1:T(8,128)(2,1)S(1)} copy(bf16[128,2,2048]{2,0,1:T(8,128)(2,1)} %bitcast.96) | data formatting | bytes 2097152 | tf_op jit(solution)/shard_map/reshape | solution.py:117
  55.2 12.5 %all-to-all-done.4 = f32[16,32,256]{2,1,0:T(8,128)S(1)} async-done(((f32[16,32,256]{2,1,0:T(8,128)}), f32[16,32,256]{2,1,0:T(8,128)S(1)}, u32[]{:S(2)}, u32[]{:S(2)}) %all-to-all-start.4) | async-done | bytes 524320 | tf_op jit(solution)/shard_map/all_to_all | solution.py:98
  67.8 0.3 copy.100
  68.1 1.0 fusion.37
  69.2 2.7 %convolution_bitcast_fusion = f32[4096,256]{0,1:T(8,128)} fusion(bf16[128,256]{1,0:T(8,128)(2,1)S(1)} %convert_element_type.17, bf16[128,4096]{0,1:T(8,128)(2,1)S(1)} %bitcast.80), kind=kOutput, calls=%fused_computation.6 | convolution fusion | flops 268435456 | bytes 5308416 | tf_op jit(solution)/shard_map/td,tc->dc/dot_general | solution.py:119
  71.9 0.0 reduce-scatter.2.cloned.1.call-update
  71.9 14.0 %all_to_all.29 = bf16[16,32,256]{2,1,0:T(8,128)(2,1)S(1)} all-to-all(bf16[16,32,256]{2,1,0:T(8,128)(2,1)S(1)} %get-tuple-element.36), channel_id=1, replica_groups=mesh['kv'=16,'tp'=2] {'kv'}, dimensions={0} | all-to-all | bytes 524288 | tf_op jit(solution)/shard_map/all_to_all | solution.py:43
  86.0 0.6 gather_fusion.3
  86.5 0.1 reshape.135
  86.7 3.6 %fusion = (f32[2,64,2,8]{1,3,2,0:T(8,128)S(1)}, f32[2,2,512,64,8]{2,3,4,1,0:T(8,128)S(1)}) fusion(f32[2,2,512,64,8]{2,3,4,1,0:T(8,128)} %copy-done, f32[2,64,2,8]{1,3,2,0:T(8,128)S(1)} %copy.73, pred[2,64,512]{2,1,0:T(8,128)(4,1)S(1)} %broadcast_compare_fusion, bf16[2,64,2,8,128]{4,3,2,1,0:T(8,128)(2,1)S(1)} %bitcast.84, ...), kind=kOutput, calls=%fused_computation.9 | convolution fusion | flops 273676288 | bytes 9519104 | tf_op jit(solution)/shard_map/bqngd,bjnd->bqngj/dot_general | solution.py:63
  90.3 0.3 copy-done.1
  90.6 1.5 fusion.2
  92.1 0.9 fusion.13
  93.0 1.8 %copy.79 = f32[2,512,2,128]{3,2,1,0:T(2,128)} copy(f32[2,512,2,128]{3,1,2,0:T(8,128)S(1)} %fusion.13) | data formatting | bytes 2097152 | tf_op jit(solution)/shard_map/mul | solution.py:73
  94.8 3.0 %reshape.138 = f32[32,8192]{1,0:T(8,128)} reshape(f32[2,512,2,128]{3,2,1,0:T(2,128)} %copy.79) | data formatting | bytes 2097152 | tf_op jit(solution)/shard_map/reshape | solution.py:84
  97.8 1.8 %fusion.28 = f32[20,8192]{1,0:T(8,128)S(1)} fusion(f32[32,8192]{1,0:T(8,128)} %reshape.138, s32[32]{0:T(128)S(1)} %eq.46), kind=kOutput, calls=%fused_computation.44 | convolution fusion | flops 62915200 | bytes 1704064 | tf_op jit(solution)/shard_map/dot_general | solution.py:82
  99.7 1.0 copy.97
  100.7 4.2 %all-to-all-start.3 = ((f32[16,32,256]{2,1,0:T(8,128)}), f32[16,32,256]{2,1,0:T(8,128)}, u32[]{:S(2)}, u32[]{:S(2)}) async-start(f32[16,32,256]{2,1,0:T(8,128)} %bitcast.88), calls=%async_computation.3 | async-start | bytes 1048576 | tf_op jit(solution)/shard_map/all_to_all | solution.py:97
  104.9 0.7 fusion.17
  105.7 0.6 copy.77
  106.3 1.1 reshape.137
  107.4 0.7 reshape.145
  108.2 17.0 %all-to-all-done.3 = f32[16,32,256]{2,1,0:T(8,128)} async-done(((f32[16,32,256]{2,1,0:T(8,128)}), f32[16,32,256]{2,1,0:T(8,128)}, u32[]{:S(2)}, u32[]{:S(2)}) %all-to-all-start.3) | async-done | bytes 524320 | tf_op jit(solution)/shard_map/all_to_all | solution.py:97
  125.2 1.4 copy.98
  126.6 0.4 convolution_add_fusion.1
  127.0 0.7 reshape.141
  127.7 24.4 %reduce-scatter.2.cloned.1.call-done = f32[256,256]{0,1:T(8,128)} async-done(((f32[4096,256]{0,1:T(8,128)}), f32[256,256]{0,1:T(8,128)}) %reduce-scatter.2.cloned.1.call-update) | async-done | bytes 262160 | tf_op jit(solution)/shard_map/reduce_scatter | solution.py:118
  152.1 1.8 %copy.83 = f32[256,256]{1,0:T(8,128)} copy(f32[256,256]{0,1:T(8,128)} %reduce-scatter.2.cloned.1.call-done) | data formatting | bytes 524288
  (29 shorter events, 0.3 us)
Async XLA Ops:
  7.2 34.2 %copy-start.6 = (bf16[128,256]{1,0:T(8,128)(2,1)S(1)}, bf16[128,256]{1,0:T(8,128)(2,1)}, u32[]{:S(2)}) copy-start(bf16[128,256]{1,0:T(8,128)(2,1)} %param.8) | copy-start | bytes 196612
  7.2 26.5 %copy-start.9 = (bf16[128,2048]{1,0:T(8,128)(2,1)S(1)}, bf16[128,2048]{1,0:T(8,128)(2,1)}, u32[]{:S(2)}) copy-start(bf16[128,2048]{1,0:T(8,128)(2,1)} %param.11) | copy-start | bytes 1572868
  7.2 46.4 %all-gather.3.cloned.1.call-start = ((), (), s32[]{:S(2)}) async-start(), calls=%async_computation.7 | async-start | bytes 1572864 | tf_op jit(solution)/shard_map/all_gather | solution.py:116
  9.4 13.8 %all-to-all-start = ((s32[16,1,1]{2,1,0:T(1,128)}), s32[16,1,1]{2,1,0:T(1,128)S(1)}, u32[]{:S(2)}, u32[]{:S(2)}) async-start(s32[16,1,1]{2,1,0:T(1,128)} %copy.70), calls=%async_computation | async-start | bytes 16384 | tf_op jit(solution)/shard_map/all_to_all | solution.py:30
  27.9 13.5 %all-to-all-start.1 = ((bf16[16,32,256]{2,1,0:T(8,128)(2,1)}), bf16[16,32,256]{2,1,0:T(8,128)(2,1)S(1)}, u32[]{:S(2)}, u32[]{:S(2)}) async-start(bf16[16,32,256]{2,1,0:T(8,128)(2,1)} %get-tuple-element.35), calls=%async_computation.1 | async-start | bytes 524288 | tf_op jit(solution)/shard_map/all_to_all | solution.py:42
  33.7 9.2 %copy-start.2 = (bf16[16,8,16,128]{3,2,1,0:T(8,128)(2,1)}, bf16[16,8,16,128]{3,2,1,0:T(8,128)(2,1)S(1)}, u32[]{:S(2)}) copy-start(bf16[16,8,16,128]{3,2,1,0:T(8,128)(2,1)S(1)} %copy.95) | copy-start | bytes 1572868
  33.8 9.1 %copy-start.4 = (bf16[16,8,16,128]{3,2,1,0:T(8,128)(2,1)}, bf16[16,8,16,128]{3,2,1,0:T(8,128)(2,1)S(1)}, u32[]{:S(2)}) copy-start(bf16[16,8,16,128]{3,2,1,0:T(8,128)(2,1)S(1)} %copy.96) | copy-start | bytes 1572868
  42.9 2.0 %copy-start = (f32[2,2,512,64,8]{2,3,4,1,0:T(8,128)}, f32[2,2,512,64,8]{2,3,4,1,0:T(8,128)S(1)}, u32[]{:S(2)}) copy-start(f32[2,2,512,64,8]{2,3,4,1,0:T(8,128)S(1)} %fusion.20) | copy-start | bytes 12582916
  49.9 17.8 %all-to-all-start.4 = ((f32[16,32,256]{2,1,0:T(8,128)}), f32[16,32,256]{2,1,0:T(8,128)S(1)}, u32[]{:S(2)}, u32[]{:S(2)}) async-start(f32[16,32,256]{2,1,0:T(8,128)} %bitcast.34), calls=%async_computation.4 | async-start | bytes 1048576 | tf_op jit(solution)/shard_map/all_to_all | solution.py:98
  53.5 98.6 %reduce-scatter.2.cloned.1.call-start = ((), (), s32[]{:S(2)}) async-start(), calls=%async_computation.6 | async-start | bytes 4456448 | tf_op jit(solution)/shard_map/reduce_scatter | solution.py:118
  69.1 16.8 %copy-start.7 = (bf16[128,256]{1,0:T(8,128)(2,1)S(1)}, bf16[128,256]{1,0:T(8,128)(2,1)}, u32[]{:S(2)}) copy-start(bf16[128,256]{1,0:T(8,128)(2,1)} %param.9) | copy-start | bytes 196612
  71.9 14.8 %copy-start.5 = (bf16[16,8,16,128]{3,2,1,0:T(8,128)(2,1)S(1)}, bf16[16,8,16,128]{3,2,1,0:T(8,128)(2,1)}, u32[]{:S(2)}) copy-start(bf16[16,8,16,128]{3,2,1,0:T(8,128)(2,1)} %copy-done.4) | copy-start | bytes 1572868
  86.7 3.9 %copy-start.1 = (f32[2,2,512,64,8]{2,3,4,1,0:T(8,128)S(1)}, f32[2,2,512,64,8]{2,3,4,1,0:T(8,128)}, u32[]{:S(2)}) copy-start(f32[2,2,512,64,8]{2,3,4,1,0:T(8,128)} %copy-done) | copy-start | bytes 12582916
  90.6 1.5 copy-start.3
  100.7 24.5 %all-to-all-start.3 = ((f32[16,32,256]{2,1,0:T(8,128)}), f32[16,32,256]{2,1,0:T(8,128)}, u32[]{:S(2)}, u32[]{:S(2)}) async-start(f32[16,32,256]{2,1,0:T(8,128)} %bitcast.88), calls=%async_computation.3 | async-start | bytes 1048576 | tf_op jit(solution)/shard_map/all_to_all | solution.py:97
  104.9 2.5 %copy-start.8 = (f32[4,8192]{1,0:T(4,128)S(1)}, f32[4,8192]{1,0:T(4,128)}, u32[]{:S(2)}) copy-start(f32[4,8192]{1,0:T(4,128)} %get-tuple-element.40) | copy-start | bytes 393220
Sparse Core Ops, SparseCore 0:
  9.5 23.9 all-gather.2
  72.0 80.0 reduce-scatter.1
